TPU v7x, 256 devices: a whole 4x4x8 slice. The times are simulated.
256 devices in a mesh: sp: 64 (over z, y, core), tp: 4 (over x).
Axes of the slice: x: 4, y: 4, z: 8, core: 2. Of those that a mesh axis runs over, the one named last changes fastest.
Arguments:
- queries: bfloat16 [8192, 2048], P('sp', 'tp'), may hold values from -6 to 6
- forget_logits: bfloat16 [2, 8192, 2048], P(None, 'sp', 'tp'), may hold values from -7.5 to 7.5
- value_matrix: bfloat16 [8192, 2048], P('sp', 'tp'), may hold values from -6 to 6
- output_gate_logits: bfloat16 [8192, 2048], P('sp', 'tp'), may hold values from -6 to 6
- forget_slack: float32 [2048], P('tp'), may hold values from 6.1035156e-05 to 0.07
- spike_log_forget: float32 [8192, 16], P('sp', 'tp'), may hold values from -2.8 to 0, as said below
- head_norm_gain: bfloat16 [128], replicated, may hold values from 0.099609375 to 1.8984375
- output_weight: bfloat16 [2048, 2048], P('tp'), may hold values from -0.125 to 0.125
- residual: bfloat16 [8192, 2048], P('sp'), may hold values from -6 to 6
- mixer_norm_gain: bfloat16 [2048], replicated, may hold values from 0.099609375 to 1.8984375
- mixer_gate_weight: bfloat16 [2048, 5632], P('sp', 'tp'), may hold values from -0.125 to 0.125
- mixer_up_weight: bfloat16 [2048, 5632], P('sp', 'tp'), may hold values from -0.125 to 0.125
- mixer_down_weight: bfloat16 [5632, 2048], P('tp', 'sp'), may hold values from -0.078125 to 0.078125
Outputs:
- layer_out: bfloat16 [8192, 2048], P(('sp', 'tp'))
Inputs may be any that keep to these rules, and one draw needn't show every extreme that they name: `spike_log_forget`: zero at all but a few tokens.
All inputs are finite; a program needn't handle non-finite values.
Results may differ from a plain program's by a relative error of at most 0.015.
Values may be sent and summed in bfloat16 or wider, within the bound.
No kernel may reach another device: no remote copies, remote signals or barrier semaphores. Data moves between devices by JAX's collectives and lax.ppermute only.
A program may use at most 128 MiB of HBM per device.

v0:
```python
import jax
import jax.numpy as jnp
from jax import lax
from jax.sharding import Mesh
from jax.sharding import PartitionSpec as P

BLOCK = 128
SP = ("sp_0", "sp_1", "sp_2")
SP_TP = ("sp_0", "sp_1", "sp_2", "tp")
NORM_EPS = 1e-06
BEST_PRECISION = lax.Precision.HIGHEST


def in_one_piece(arrays, axis, dim, along):
    both = jnp.concatenate(arrays, axis=along)
    whole, at, gathered = (lax.all_gather(both, axis, axis=dim, tiled=True), 0, [])
    for a in arrays:
        gathered.append(lax.slice_in_dim(whole, at, at + a.shape[along], axis=along))
        at += a.shape[along]
    return tuple(gathered)


def in_order(pieces, dim):
    dims = list(pieces.shape[1:])
    dims[dim] *= pieces.shape[0]
    return jnp.moveaxis(pieces, 0, dim).reshape(dims)


def gather_in_order(array, axes, order):
    pieces = array[None]
    for k in order:
        pieces = lax.all_gather(pieces, axes[k], axis=0, tiled=True)
    block = [lax.axis_size(axes[k]) for k in reversed(order)]
    pieces = pieces.reshape(*block, *array.shape)
    turned = sorted(range(len(order)), key=lambda place: order[len(order) - 1 - place])
    return pieces.transpose(*turned, *range(len(order), pieces.ndim)).reshape(-1, *array.shape)


def gathered_by_axis(array, axes, order, dim):
    return in_order(gather_in_order(array, axes, order), dim)


def neutral_like(array, identity):
    return jax.tree.map(
        lambda a, e: jnp.broadcast_to(jnp.asarray(e, a.dtype), a.shape), array, identity
    )


def carried_in(array, axes, combine, identity, reverse):
    before = start = neutral_like(array, identity)
    subtotal = array
    for axis in reversed(axes):
        size, position = (lax.axis_size(axis), lax.axis_index(axis))
        pieces = jax.tree.map(
            lambda part, kind: lax.all_gather(part.astype(kind), axis),
            subtotal,
            (jnp.bfloat16, jnp.bfloat16),
        )
        inside, subtotal = (start, start)
        for k in reversed(range(size)) if reverse else range(size):
            passed = k > position if reverse else k < position
            subtotal = combine(
                subtotal, jax.tree.map(lambda part, own: part[k].astype(own.dtype), pieces, array)
            )
            inside = jax.tree.map(lambda new, old: jnp.where(passed, new, old), subtotal, inside)
        before = combine(inside, before)
    return before


def in_blocks(array, dim, size):
    dims = array.shape
    pieces = array.reshape(*dims[:dim], size, dims[dim] // size, *dims[dim + 1 :])
    return jnp.moveaxis(pieces, dim, 0)


def summed_on_arrival(array, axis, dim):
    size = lax.axis_size(axis)
    pieces = lax.all_to_all(in_blocks(array, dim, size), axis, 0, 0, tiled=True)
    return jnp.sum(pieces.astype(jnp.float32), axis=0)


def from_everyone(array, axis):
    copies = jnp.broadcast_to(array, (lax.axis_size(axis), *array.shape))
    return lax.all_to_all(copies, axis, split_axis=0, concat_axis=0, tiled=True)


def gathered_copies(array, axis, dim):
    return in_order(from_everyone(array, axis), dim)


def rms_scale(entries, gain_vec):
    return (
        entries
        * lax.rsqrt(jnp.mean(entries * entries, axis=-1, keepdims=True) + NORM_EPS)
        * gain_vec.astype(jnp.float32)
    )


def reverse_rows(tensor):
    return jnp.flip(tensor, 0)


def local_sweep(query_f, key_f, decay_f, value_f):
    row_count, heads_present, head_width = query_f.shape
    blocks_count = row_count // BLOCK
    tri_mask = jnp.tril(jnp.ones((BLOCK, BLOCK), bool))

    def to_blocks(tensor):
        return tensor.reshape(blocks_count, BLOCK, heads_present, head_width)

    def advance(carried, segment):
        state_now, offset = carried
        query_seg, key_seg, decay_seg, value_seg = segment
        running = jnp.cumsum(decay_seg, axis=0)
        query_scaled = query_seg * jnp.exp(running)
        key_scaled = key_seg * jnp.exp(-running)
        scores = jnp.einsum("thd,shd->hts", query_scaled, key_scaled, precision=BEST_PRECISION)
        scores = jnp.where(tri_mask[None], scores, 0.0)
        result = jnp.einsum("hts,shv->thv", scores, value_seg, precision=BEST_PRECISION)
        result = result + jnp.einsum(
            "thd,hdv->thv", query_scaled, state_now, precision=BEST_PRECISION
        )
        final_log = running[-1]
        state_next = jnp.exp(final_log)[:, :, None] * state_now + jnp.einsum(
            "shd,shv->hdv",
            key_seg * jnp.exp(final_log[None] - running),
            value_seg,
            precision=BEST_PRECISION,
        )
        reach = query_seg * jnp.exp(running + offset)
        return ((state_next, offset + final_log), (result, reach))

    initial = (
        jnp.zeros((heads_present, head_width, head_width), jnp.float32),
        jnp.zeros((heads_present, head_width), jnp.float32),
    )
    (state_end, offset_end), (results, reaches) = lax.scan(
        advance,
        initial,
        (to_blocks(query_f), to_blocks(key_f), to_blocks(decay_f), to_blocks(value_f)),
    )
    shape_back = (row_count, heads_present, head_width)
    return (
        results.reshape(shape_back),
        reaches.reshape(shape_back),
        state_end,
        jnp.exp(offset_end),
    )


def chain(earlier, latter):
    return (earlier[0] * latter[0], latter[0][..., None] * earlier[1] + latter[1])


def local(
    queries,
    forget_logits,
    value_matrix,
    output_gate_logits,
    forget_slack,
    spike_log_forget,
    head_norm_gain,
    output_weight,
    residual,
    mixer_norm_gain,
    mixer_gate_weight,
    mixer_up_weight,
    mixer_down_weight,
):
    gate_whole, up_whole = in_one_piece((mixer_gate_weight, mixer_up_weight), SP, 0, 1)
    down_whole = gathered_by_axis(mixer_down_weight, SP, (1, 0, 2), 1)
    row_count = queries.shape[0]
    heads_present = spike_log_forget.shape[1]
    head_width = queries.shape[1] // heads_present
    query_f = (jax.nn.silu(queries.astype(jnp.float32)) * head_width ** (-0.5)).reshape(
        row_count, heads_present, head_width
    )
    value_f = value_matrix.astype(jnp.float32).reshape(row_count, heads_present, head_width)
    gate_random_key = (forget_slack * jax.nn.sigmoid(-forget_logits.astype(jnp.float32))).reshape(
        2, row_count, heads_present, head_width
    )
    decay_logarithm = jnp.log1p(-gate_random_key) + spike_log_forget[None, :, :, None]
    fore_local, fore_reach, fore_state, fore_total = local_sweep(
        query_f, gate_random_key[0], decay_logarithm[0], value_f
    )
    back_local, back_reach, back_state, back_total = local_sweep(
        reverse_rows(query_f),
        reverse_rows(gate_random_key[1]),
        reverse_rows(decay_logarithm[1]),
        reverse_rows(value_f),
    )
    neutral = (jnp.ones_like(fore_total), jnp.zeros_like(fore_state))
    _, fore_enter = carried_in((fore_total, fore_state), SP, chain, neutral, False)
    _, back_enter = carried_in((back_total, back_state), SP, chain, neutral, True)
    fore_out = fore_local + jnp.einsum(
        "thd,hdv->thv", fore_reach, fore_enter, precision=BEST_PRECISION
    )
    back_out = back_local + jnp.einsum(
        "thd,hdv->thv", back_reach, back_enter, precision=BEST_PRECISION
    )
    mixture = fore_out + reverse_rows(back_out)
    mixed = (
        rms_scale(mixture, head_norm_gain).reshape(row_count, heads_present * head_width)
        * jax.nn.silu(output_gate_logits.astype(jnp.float32))
    ).astype(jnp.bfloat16)
    part_rows = row_count // lax.axis_size("tp")
    own_start = lax.axis_index("tp") * part_rows
    partial_out = jnp.dot(mixed, output_weight, preferred_element_type=jnp.float32).astype(
        jnp.bfloat16
    )
    mixer_add = summed_on_arrival(
        lax.optimization_barrier(partial_out).astype(jnp.float32).astype(jnp.bfloat16), "tp", 0
    )
    own_resid = lax.dynamic_slice_in_dim(residual, own_start, part_rows, 0)
    hidden_state = (own_resid.astype(jnp.float32) + mixer_add).astype(jnp.bfloat16)
    normed_part = rms_scale(hidden_state.astype(jnp.float32), mixer_norm_gain).astype(jnp.bfloat16)
    normed = gathered_copies(normed_part, "tp", 0)
    gate_act = jnp.dot(normed, gate_whole, preferred_element_type=jnp.float32)
    up_act = jnp.dot(normed, up_whole, preferred_element_type=jnp.float32)
    inner = (jax.nn.silu(gate_act) * up_act).astype(jnp.bfloat16)
    lowered = jnp.dot(inner, down_whole, preferred_element_type=jnp.float32)
    lowered_term = lax.optimization_barrier(lowered.astype(jnp.bfloat16)).astype(jnp.float32)
    ffn_add = summed_on_arrival(lowered_term.astype(jnp.bfloat16), "tp", 0)
    return (hidden_state.astype(jnp.float32) + ffn_add).astype(jnp.bfloat16)


def solution(mesh):
    torus = Mesh(mesh.devices.reshape(8, 4, 2, mesh.shape["tp"]), ("sp_0", "sp_1", "sp_2", "tp"))
    return jax.shard_map(
        local,
        mesh=torus,
        in_specs=(
            P(SP, "tp"),
            P(None, SP, "tp"),
            P(SP, "tp"),
            P(SP, "tp"),
            P("tp"),
            P(SP, "tp"),
            P(),
            P("tp", None),
            P(SP, None),
            P(),
            P(SP, "tp"),
            P(SP, "tp"),
            P("tp", SP),
        ),
        out_specs=P(SP_TP, None),
        check_vma=False,
    )
```

profile of v0, /device:TPU:1, one launch (start us, length us, event | category | flops | bytes accessed | tf_op | source)
XLA Modules:
  0.0 290.6 jit_solution(12369992402076362102)
XLA Ops:
  6.5 12.1 %all-gather.2 = bf16[5632,32]{0,1:T(8,128)(2,1)S(1)} all-gather(bf16[1408,32]{0,1:T(8,128)(2,1)} %param.25), channel_id=4, replica_groups=mesh['sp_0'=8,'sp_1'=4,'sp_2'=2,'tp'=4] {'sp_1'}, dimensions={0}, use_global_device_ids=true | all-gather | bytes 450560 | tf_op jit(solution)/shard_map/all_gather | solution.py:32
  18.7 0.8 copy.172
  19.5 1.2 divide_multiply_fusion
  20.8 0.8 squeeze.39
  21.6 1.0 log1p.7
  22.6 0.8 copy.111
  23.4 1.2 broadcast_add_fusion
  24.7 1.0 fusion.40
  25.7 0.8 squeeze.37
  26.5 0.8 squeeze.43
  27.3 0.1 rev.19
  27.4 0.1 fusion.93
  27.6 0.1 fusion.276
  27.7 5.7 %all_gather.71 = bf16[2,4,128]{2,1,0:T(4,128)(2,1)S(1)} all-gather(bf16[1,4,128]{2,1,0:T(4,128)(2,1)S(1)} %get-tuple-element.86), channel_id=1, replica_groups=mesh['sp_0'=8,'sp_1'=4,'sp_2'=2,'tp'=4] {'sp_2'}, dimensions={0}, use_global_device_ids=true | all-gather | bytes 3072 | tf_op jit(solution)/shard_map/all_gather | solution.py:55
  33.4 6.6 %all_gather.72 = bf16[4,4,128]{2,1,0:T(4,128)(2,1)S(1)} all-gather(bf16[1,4,128]{2,1,0:T(4,128)(2,1)S(1)} %fusion.242), channel_id=1, replica_groups=mesh['sp_0'=8,'sp_1'=4,'sp_2'=2,'tp'=4] {'sp_1'}, dimensions={0}, use_global_device_ids=true | all-gather | bytes 5120 | tf_op jit(solution)/shard_map/all_gather | solution.py:55
  40.0 2.4 exponential_multiply_fusion.3
  42.5 0.6 fusion.16
  43.1 3.6 %all-gather.1 = bf16[8,128,128]{2,1,0:T(8,128)(2,1)S(1)} all-gather(bf16[4,128,128]{2,1,0:T(8,128)(2,1)S(1)} %fusion.16), channel_id=3, replica_groups=mesh['sp_0'=8,'sp_1'=4,'sp_2'=2,'tp'=4] {'sp_2'}, dimensions={0}, use_global_device_ids=true | all-gather | bytes 393216 | tf_op jit(solution)/shard_map/all_gather | solution.py:55
  46.7 0.6 fusion.251
  47.4 0.2 fusion.88
  47.6 11.1 %all_gather.76 = bf16[4,4,128,128]{3,2,1,0:T(8,128)(2,1)S(1)} all-gather(bf16[1,4,128,128]{3,2,1,0:T(8,128)(2,1)S(1)} %fusion.88), channel_id=1, replica_groups=mesh['sp_0'=8,'sp_1'=4,'sp_2'=2,'tp'=4] {'sp_1'}, dimensions={0}, use_global_device_ids=true | all-gather | bytes 655360 | tf_op jit(solution)/shard_map/all_gather | solution.py:55
  58.7 0.6 copy-done.11
  59.3 1.0 fusion.74
  60.4 3.5 %all_gather.64 = bf16[2,4,128]{2,1,0:T(4,128)(2,1)S(1)} all-gather(bf16[1,4,128]{2,1,0:T(4,128)(2,1)S(1)} %get-tuple-element.113), channel_id=1, replica_groups=mesh['sp_0'=8,'sp_1'=4,'sp_2'=2,'tp'=4] {'sp_2'}, dimensions={0}, use_global_device_ids=true | all-gather | bytes 3072 | tf_op jit(solution)/shard_map/all_gather | solution.py:55
  63.9 5.9 %all_gather.65 = bf16[4,4,128]{2,1,0:T(4,128)(2,1)S(1)} all-gather(bf16[1,4,128]{2,1,0:T(4,128)(2,1)S(1)} %fusion.240), channel_id=1, replica_groups=mesh['sp_0'=8,'sp_1'=4,'sp_2'=2,'tp'=4] {'sp_1'}, dimensions={0}, use_global_device_ids=true | all-gather | bytes 5120 | tf_op jit(solution)/shard_map/all_gather | solution.py:55
  69.9 0.7 exponential_multiply_fusion.7
  70.6 1.4 fusion.15
  71.9 3.7 %all-gather = bf16[8,128,128]{2,1,0:T(8,128)(2,1)S(1)} all-gather(bf16[4,128,128]{2,1,0:T(8,128)(2,1)S(1)} %fusion.15), channel_id=2, replica_groups=mesh['sp_0'=8,'sp_1'=4,'sp_2'=2,'tp'=4] {'sp_2'}, dimensions={0}, use_global_device_ids=true | all-gather | bytes 393216 | tf_op jit(solution)/shard_map/all_gather | solution.py:55
  75.7 0.7 fusion.246
  76.4 0.2 fusion.84
  76.6 9.9 %all_gather.69 = bf16[4,4,128,128]{3,2,1,0:T(8,128)(2,1)S(1)} all-gather(bf16[1,4,128,128]{3,2,1,0:T(8,128)(2,1)S(1)} %fusion.84), channel_id=1, replica_groups=mesh['sp_0'=8,'sp_1'=4,'sp_2'=2,'tp'=4] {'sp_1'}, dimensions={0}, use_global_device_ids=true | all-gather | bytes 655360 | tf_op jit(solution)/shard_map/all_gather | solution.py:55
  86.5 0.8 copy-done.1
  87.3 1.0 fusion.56
  88.4 0.5 all-gather.17.cloned.1.call-update
  89.0 1.6 pad_maximum_fusion
  90.6 1.2 convert_element_type.813
  91.9 15.8 %all_gather.73 = bf16[8,4,128]{2,1,0:T(4,128)(2,1)S(1)} all-gather(bf16[1,4,128]{2,1,0:T(4,128)(2,1)S(1)} %fusion.252), channel_id=1, replica_groups=mesh['sp_0'=8,'sp_1'=4,'sp_2'=2,'tp'=4] {'sp_0'}, dimensions={0}, use_global_device_ids=true | all-gather | bytes 9216 | tf_op jit(solution)/shard_map/all_gather | solution.py:55
  107.7 9.8 %all_gather.66 = bf16[8,4,128]{2,1,0:T(4,128)(2,1)S(1)} all-gather(bf16[1,4,128]{2,1,0:T(4,128)(2,1)S(1)} %fusion.247), channel_id=1, replica_groups=mesh['sp_0'=8,'sp_1'=4,'sp_2'=2,'tp'=4] {'sp_0'}, dimensions={0}, use_global_device_ids=true | all-gather | bytes 9216 | tf_op jit(solution)/shard_map/all_gather | solution.py:55
  117.6 0.6 fusion.259
  118.2 0.6 fusion.266
  118.8 1.6 convolution_select_fusion.1
  120.4 0.4 convolution_bitcast_fusion.5
  120.9 1.6 convolution_select_fusion
  122.5 0.6 convolution_bitcast_fusion.2
  123.2 1.4 fusion.11
  124.5 1.4 fusion.14
  125.9 4.2 %fusion.10 = f32[128,4,128]{0,2,1:T(8,128)} fusion(f32[128,4,128]{0,2,1:T(8,128)} %fusion.11, f32[128,4,128]{2,1,0:T(4,128)S(1)} %get-tuple-element.68, bf16[8,4,128,128]{3,2,1,0:T(8,128)(2,1)} %all-gather.11.cloned.1.call-done, f32[4,128]{1,0:T(4,128)S(1)} %get-tuple-element.110, f32[4,128]{1,0:T(4,128)} %copy-done.7, f32[4,128]{1,0:T(4,128)} %copy-done.9, ...), kind=kOutput, calls=%fused_computation.9 | convolution fusion | flops 104464384 | bytes 2654222 | tf_op jit(solution)/shard_map/thd,hdv->thv/dot_general | solution.py:198
  130.2 2.0 rev.20
  132.1 7.9 %all-gather.9.cloned.1.call-done = bf16[8,4,128,128]{3,2,1,0:T(8,128)(2,1)} async-done(((bf16[1,4,128,128]{3,2,1,0:T(8,128)(2,1)}), bf16[8,4,128,128]{3,2,1,0:T(8,128)(2,1)}) %all-gather.9.cloned.1.call-update) | async-done | bytes 1048592 | tf_op jit(solution)/shard_map/all_gather | solution.py:55
  140.1 3.7 %multiply_reduce_fusion = (f32[128,4]{0,1:T(4,128)S(1)}, f32[128,4,128]{0,2,1:T(8,128)S(1)}) fusion(f32[128,4,128]{0,2,1:T(8,128)S(1)} %rev.20, f32[128,4,128]{0,2,1:T(8,128)} %fusion.14, f32[128,4,128]{2,1,0:T(4,128)S(1)} %get-tuple-element.67, bf16[8,4,128,128]{3,2,1,0:T(8,128)(2,1)} %all-gather.9.cloned.1.call-done, ...), kind=kOutput, calls=%fused_computation.172 | convolution fusion | flops 104660480 | bytes 2918414 | tf_op jit(solution)/shard_map/thd,hdv->thv/dot_general | solution.py:195
  143.8 0.1 copy.130
  144.0 1.3 convolution_convert_fusion
  145.3 3.9 %all-to-all-start = ((bf16[4,32,2048]{2,1,0:T(8,128)(2,1)}), bf16[4,32,2048]{2,1,0:T(8,128)(2,1)S(1)}, u32[]{:S(2)}, u32[]{:S(2)}) async-start(bf16[4,32,2048]{2,1,0:T(8,128)(2,1)} %bitcast.67), calls=%async_computation | async-start | bytes 1048576 | tf_op jit(solution)/shard_map/all_to_all | solution.py:78
  149.2 6.9 %all-to-all-done = bf16[4,32,2048]{2,1,0:T(8,128)(2,1)S(1)} async-done(((bf16[4,32,2048]{2,1,0:T(8,128)(2,1)}), bf16[4,32,2048]{2,1,0:T(8,128)(2,1)S(1)}, u32[]{:S(2)}, u32[]{:S(2)}) %all-to-all-start) | async-done | bytes 524320 | tf_op jit(solution)/shard_map/all_to_all | solution.py:78
  156.2 1.1 fusion.89
  157.4 0.9 broadcast_in_dim.106
  158.3 3.7 %all-to-all-start.1 = ((bf16[4,32,2048]{2,1,0:T(8,128)(2,1)}), bf16[4,32,2048]{2,1,0:T(8,128)(2,1)S(1)}, u32[]{:S(2)}, u32[]{:S(2)}) async-start(bf16[4,32,2048]{2,1,0:T(8,128)(2,1)} %broadcast_in_dim.106), calls=%async_computation.1 | async-start | bytes 1048576 | tf_op jit(solution)/shard_map/all_to_all | solution.py:84
  162.0 5.2 %all-gather.17.cloned.1.call-done = bf16[64,1408,32]{1,2,0:T(8,128)(2,1)} async-done(((bf16[32,1408,32]{1,2,0:T(8,128)(2,1)}), bf16[64,1408,32]{1,2,0:T(8,128)(2,1)}) %all-gather.17.cloned.1.call-update) | async-done | bytes 5767184 | tf_op jit(solution)/shard_map/all_gather | solution.py:32
  167.2 5.9 %copy.132 = bf16[8,4,2,1408,32]{3,4,2,1,0:T(8,128)(2,1)} copy(bf16[8,4,2,1408,32]{3,4,1,0,2:T(8,128)(2,1)} %bitcast.511) | data formatting | bytes 11534336 | tf_op jit(solution)/shard_map/transpose | solution.py:36
  173.1 85.4 %all-gather.13.cloned.1.call-done = bf16[2048,2816]{1,0:T(8,128)(2,1)} async-done(((bf16[32,2816]{1,0:T(8,128)(2,1)}), bf16[2048,2816]{1,0:T(8,128)(2,1)}) %all-gather.13.cloned.1.call-update) | async-done | bytes 11534352 | tf_op jit(solution)/shard_map/all_gather | solution.py:16
  258.5 4.5 %fusion.2 = f32[128,1408]{1,0:T(8,128)} fusion(bf16[128,2048]{1,0:T(8,128)(2,1)S(1)} %bitcast.516, bf16[2048,2816]{1,0:T(8,128)(2,1)} %all-gather.13.cloned.1.call-done), kind=kOutput, calls=%fused_computation.2 | convolution fusion | flops 738197504 | bytes 7012352 | tf_op jit(solution)/shard_map/dot_general | solution.py:218
  263.1 7.4 %convolution_convert_fusion.1 = bf16[128,2048]{1,0:T(8,128)(2,1)S(1)} fusion(bf16[1408,2048]{0,1:T(8,128)(2,1)} %bitcast.512, bf16[128,2048]{1,0:T(8,128)(2,1)S(1)} %bitcast.517, bf16[2048,2816]{1,0:T(8,128)(2,1)} %all-gather.13.cloned.1.call-done, f32[128,1408]{1,0:T(8,128)} %fusion.2), kind=kOutput, calls=%fused_computation.7 | convolution fusion | flops 1477738496 | bytes 13303808 | tf_op jit(solution)/shard_map/dot_general | solution.py:221
  270.5 12.8 %all_to_all.15 = bf16[4,32,2048]{2,1,0:T(8,128)(2,1)S(1)} all-to-all(bf16[4,32,2048]{2,1,0:T(8,128)(2,1)S(1)} %bitcast.518), channel_id=1, replica_groups=mesh['sp_0'=8,'sp_1'=4,'sp_2'=2,'tp'=4] {'tp'}, dimensions={0} | all-to-all | bytes 1048576 | tf_op jit(solution)/shard_map/all_to_all | solution.py:78
  283.4 0.7 fusion.92
  (88 shorter events, 1.0 us)
Async XLA Ops:
  6.5 137.5 %copy-start = (bf16[512,2048]{1,0:T(8,128)(2,1)S(1)}, bf16[512,2048]{1,0:T(8,128)(2,1)}, u32[]{:S(2)}) copy-start(bf16[512,2048]{1,0:T(8,128)(2,1)} %param.20) | copy-start | bytes 6291460
  6.5 20.7 %copy-start.2 = (bf16[128,512]{1,0:T(8,128)(2,1)S(1)}, bf16[128,512]{1,0:T(8,128)(2,1)}, u32[]{:S(2)}) copy-start(bf16[128,512]{1,0:T(8,128)(2,1)} %param.15) | copy-start | bytes 393220
  6.5 81.9 %all-gather.15.cloned.1.call-start = ((), (), s32[]{:S(2)}) async-start(), calls=%async_computation.6 | async-start | bytes 3244032 | tf_op jit(solution)/shard_map/all_gather | solution.py:32
  19.5 106.4 %all-gather.11.cloned.1.call-start = ((), (), s32[]{:S(2)}) async-start(), calls=%async_computation.4 | async-start | bytes 1179648 | tf_op jit(solution)/shard_map/all_gather | solution.py:55
  27.6 19.8 %copy-start.3 = (f32[128,4,128]{2,1,0:T(4,128)}, f32[128,4,128]{2,1,0:T(4,128)S(1)}, u32[]{:S(2)}) copy-start(f32[128,4,128]{2,1,0:T(4,128)S(1)} %fusion.93) | copy-start | bytes 786436
  46.7 0.7 copy-start.4
  46.7 17.2 %copy-start.7 = (f32[4,128]{1,0:T(4,128)}, f32[4,128]{1,0:T(4,128)S(1)}, u32[]{:S(2)}) copy-start(f32[4,128]{1,0:T(4,128)S(1)} %convert_bitcast_fusion.20) | copy-start | bytes 6148
  47.3 11.4 %copy-start.9 = (f32[4,128]{1,0:T(4,128)}, f32[4,128]{1,0:T(4,128)S(1)}, u32[]{:S(2)}) copy-start(f32[4,128]{1,0:T(4,128)S(1)} %get-tuple-element.105) | copy-start | bytes 6148
  58.7 0.6 copy-start.11
  58.7 0.6 copy-start.12
  58.7 0.6 copy-start.13
  60.3 79.7 %all-gather.9.cloned.1.call-start = ((), (), s32[]{:S(2)}) async-start(), calls=%async_computation.3 | async-start | bytes 1179648 | tf_op jit(solution)/shard_map/all_gather | solution.py:55
  75.7 0.7 copy-start.5
  75.7 10.8 %copy-start.8 = (f32[4,128]{1,0:T(4,128)}, f32[4,128]{1,0:T(4,128)S(1)}, u32[]{:S(2)}) copy-start(f32[4,128]{1,0:T(4,128)S(1)} %convert_bitcast_fusion.22) | copy-start | bytes 6148
  76.3 10.2 %copy-start.10 = (f32[4,128]{1,0:T(4,128)}, f32[4,128]{1,0:T(4,128)S(1)}, u32[]{:S(2)}) copy-start(f32[4,128]{1,0:T(4,128)S(1)} %get-tuple-element.101) | copy-start | bytes 6148
  86.5 0.8 copy-start.1
  86.5 0.8 copy-start.14
  86.5 0.8 copy-start.15
  86.5 0.8 copy-start.16
  88.3 78.8 %all-gather.17.cloned.1.call-start = ((), (), s32[]{:S(2)}) async-start(), calls=%async_computation.7 | async-start | bytes 8650752 | tf_op jit(solution)/shard_map/all_gather | solution.py:32
  88.9 169.6 %all-gather.13.cloned.1.call-start = ((), (), s32[]{:S(2)}) async-start(), calls=%async_computation.5 | async-start | bytes 11714560 | tf_op jit(solution)/shard_map/all_gather | solution.py:16
  120.9 19.1 %copy-start.18 = (f32[4,128]{1,0:T(4,128)S(1)}, f32[4,128]{1,0:T(4,128)}, u32[]{:S(2)}) copy-start(f32[4,128]{1,0:T(4,128)} %get-tuple-element.87) | copy-start | bytes 6148
  120.9 19.1 %copy-start.19 = (f32[4,128]{1,0:T(4,128)S(1)}, f32[4,128]{1,0:T(4,128)}, u32[]{:S(2)}) copy-start(f32[4,128]{1,0:T(4,128)} %get-tuple-element.88) | copy-start | bytes 6148
  120.9 19.1 %copy-start.20 = (f32[4,128]{1,0:T(4,128)S(1)}, f32[4,128]{1,0:T(4,128)}, u32[]{:S(2)}) copy-start(f32[4,128]{1,0:T(4,128)} %get-tuple-element.89) | copy-start | bytes 6148
  120.9 19.1 %copy-start.21 = (f32[4,128]{1,0:T(4,128)S(1)}, f32[4,128]{1,0:T(4,128)}, u32[]{:S(2)}) copy-start(f32[4,128]{1,0:T(4,128)} %get-tuple-element.90) | copy-start | bytes 6148
  120.9 19.1 %copy-start.22 = (f32[4,128]{1,0:T(4,128)S(1)}, f32[4,128]{1,0:T(4,128)}, u32[]{:S(2)}) copy-start(f32[4,128]{1,0:T(4,128)} %get-tuple-element.91) | copy-start | bytes 6148
  120.9 19.1 %copy-start.23 = (f32[4,128]{1,0:T(4,128)S(1)}, f32[4,128]{1,0:T(4,128)}, u32[]{:S(2)}) copy-start(f32[4,128]{1,0:T(4,128)} %get-tuple-element.92) | copy-start | bytes 6148
  120.9 19.1 %copy-start.24 = (f32[4,128]{1,0:T(4,128)S(1)}, f32[4,128]{1,0:T(4,128)}, u32[]{:S(2)}) copy-start(f32[4,128]{1,0:T(4,128)} %get-tuple-element.93) | copy-start | bytes 6148
  123.2 16.9 %copy-start.6 = (bf16[8,128,128]{2,1,0:T(8,128)(2,1)S(1)}, bf16[8,128,128]{2,1,0:T(8,128)(2,1)}, u32[]{:S(2)}) copy-start(bf16[8,128,128]{2,1,0:T(8,128)(2,1)} %copy-done.5) | copy-start | bytes 786436
  124.5 19.2 %copy-start.25 = (f32[128]{0:T(128)S(1)}, f32[128]{0:T(128)}, u32[]{:S(2)}) copy-start(f32[128]{0:T(128)} %convert_element_type.813) | copy-start | bytes 1540
  130.1 13.9 %copy-start.26 = (bf16[128,512]{1,0:T(8,128)(2,1)S(1)}, bf16[128,512]{1,0:T(8,128)(2,1)}, u32[]{:S(2)}) copy-start(bf16[128,512]{1,0:T(8,128)(2,1)} %param.16) | copy-start | bytes 393220
  130.1 19.1 %copy-start.17 = (bf16[2048]{0:T(1024)(128)(2,1)S(1)}, bf16[2048]{0:T(1024)(128)(2,1)}, u32[]{:S(2)}) copy-start(bf16[2048]{0:T(1024)(128)(2,1)} %param.22) | copy-start | bytes 12292
  145.3 10.9 %all-to-all-start = ((bf16[4,32,2048]{2,1,0:T(8,128)(2,1)}), bf16[4,32,2048]{2,1,0:T(8,128)(2,1)S(1)}, u32[]{:S(2)}, u32[]{:S(2)}) async-start(bf16[4,32,2048]{2,1,0:T(8,128)(2,1)} %bitcast.67), calls=%async_computation | async-start | bytes 1048576 | tf_op jit(solution)/shard_map/all_to_all | solution.py:78
  158.3 14.8 %all-to-all-start.1 = ((bf16[4,32,2048]{2,1,0:T(8,128)(2,1)}), bf16[4,32,2048]{2,1,0:T(8,128)(2,1)S(1)}, u32[]{:S(2)}, u32[]{:S(2)}) async-start(bf16[4,32,2048]{2,1,0:T(8,128)(2,1)} %broadcast_in_dim.106), calls=%async_computation.1 | async-start | bytes 1048576 | tf_op jit(solution)/shard_map/all_to_all | solution.py:84
Sparse Core Ops, SparseCore 0:
  19.6 45.9 all-gather.14
  67.4 33.8 all-gather.10
  103.2 36.8 all-gather.8
  141.7 25.4 all-gather.16
  169.8 88.7 all-gather.12
where the time goes:
time: 291 us
  waiting for transfers between devices  106 us (36%)
  blocking collectives  101 us (35%)
  matrix products  30.1 us (10%)
  other arithmetic  16.9 us (6%)
  local copies, waits for them, and re-layouts  15.6 us (5%)
  between operations  13.6 us (5%)
  starting transfers between devices  7.79 us (3%)
    all_gather x1, waiting for transfers between devices, in_one_piece(): lax.all_gather(both, axis, axis=dim, tiled=True)  85.4 us
    all_gather x10, blocking collectives, carried_in(): lax.all_gather(part.astype(kind), axis)  75.8 us
    all_to_all x1, blocking collectives, summed_on_arrival(): pieces = lax.all_to_all(in_blocks(array, dim, size), axis, 0, 0, tiled=True)  12.8 us
    all_gather x1, blocking collectives, gather_in_order(): pieces = lax.all_gather(pieces, axes[k], axis=0, tiled=True)  12.1 us
    all_gather x2, waiting for transfers between devices, carried_in(): lax.all_gather(part.astype(kind), axis)  7.87 us
    dot_general x1, matrix products, local(): lowered = jnp.dot(inner, down_whole, preferred_element_type=jnp.float32)  7.42 us
    all_to_all x1, waiting for transfers between devices, summed_on_arrival(): pieces = lax.all_to_all(in_blocks(array, dim, size), axis, 0, 0, tiled=True)  6.93 us
    transpose x1, local copies, waits for them, and re-layouts, gather_in_order(): pieces.transpose(*turned, *range(len(order), pieces.ndim))  5.92 us
  transfers between devices with their start and end apart: 7, of which 4 were waited for; matrix products, arithmetic and copies ran while one was open for 16% of the time, Pallas kernels for 0%

commit v1 on v0

--- a/solution.py
+++ b/solution.py
@@ -29,7 +29,10 @@
 def gather_in_order(array, axes, order):
     pieces = array[None]
     for k in order:
-        pieces = lax.all_gather(pieces, axes[k], axis=0, tiled=True)
+        devices = lax.axis_size(axes[k])
+        parts = jnp.stack([pieces for _ in range(devices)])
+        parts = lax.all_to_all(parts, axes[k], split_axis=0, concat_axis=0)
+        pieces = jnp.concatenate(parts, axis=0)
     block = [lax.axis_size(axes[k]) for k in reversed(order)]
     pieces = pieces.reshape(*block, *array.shape)
     turned = sorted(range(len(order)), key=lambda place: order[len(order) - 1 - place])

time: 291 us -> 305 us (1.048)
  waiting for transfers between devices: 106 us -> 81.9 us
  blocking collectives: 101 us -> 122 us
  local copies, waits for them, and re-layouts: 15.6 us -> 21.1 us
  other arithmetic: 16.9 us -> 22.4 us
  starting transfers between devices: 7.79 us -> 12.3 us
    all_gather x1, waiting for transfers between devices: 85.4 us -> 0.01 us  [in_one_piece(): lax.all_gather(both, axis, axis=dim, tiled=True)]
    all_to_all x1 -> x2, waiting for transfers between devices: 6.93 us -> 78.6 us  [gather_in_order(): parts = lax.all_to_all(parts, axes[k], split_axis=0, concat_axis=0)]
    all_to_all x0 -> x1, blocking collectives: none -> 24.7 us  [gather_in_order(): parts = lax.all_to_all(parts, axes[k], split_axis=0, concat_axis=0)]
    all_gather x1 -> x0, blocking collectives: 12.1 us -> none  [gather_in_order(): pieces = lax.all_gather(pieces, axes[k], axis=0, tiled=True)]
    all_to_all x1 -> x2, blocking collectives: 12.8 us -> 21.5 us  [summed_on_arrival(): pieces = lax.all_to_all(in_blocks(array, dim, size), axis, 0, 0, tiled=True)]
    all_gather x2, waiting for transfers between devices: 7.87 us -> 0.02 us  [carried_in(): lax.all_gather(part.astype(kind), axis)]
    all_to_all x0 -> x1, local copies, waits for them, and re-layouts: none -> 5.99 us  [gather_in_order(): parts = lax.all_to_all(parts, axes[k], split_axis=0, concat_axis=0)]
    transpose x1 -> x0, local copies, waits for them, and re-layouts: 5.92 us -> none  [gather_in_order(): pieces.transpose(*turned, *range(len(order), pieces.ndim))]
  transfers between devices with their start and end apart: 7 -> 6, of which waited for: 4 -> 2; matrix products, arithmetic and copies ran while one was open for 16% -> 14% of each run, Pallas kernels for 0% -> 0%
where the time goes in v1:
time: 305 us; the launch traced here: 304 us
  blocking collectives  122 us (40%)
  waiting for transfers between devices  81.9 us (27%)
  matrix products  30.2 us (10%)
  other arithmetic  22.4 us (7%)
  local copies, waits for them, and re-layouts  21.1 us (7%)
  between operations  13.6 us (4%)
  starting transfers between devices  12.3 us (4%)
    all_to_all x2, waiting for transfers between devices, gather_in_order(): parts = lax.all_to_all(parts, axes[k], split_axis=0, concat_axis=0)  78.6 us
    all_gather x10, blocking collectives, carried_in(): lax.all_gather(part.astype(kind), axis)  75.9 us
    all_to_all x1, blocking collectives, gather_in_order(): parts = lax.all_to_all(parts, axes[k], split_axis=0, concat_axis=0)  24.7 us
    all_to_all x2, blocking collectives, summed_on_arrival(): pieces = lax.all_to_all(in_blocks(array, dim, size), axis, 0, 0, tiled=True)  21.5 us
    all_to_all x2, starting transfers between devices, gather_in_order(): parts = lax.all_to_all(parts, axes[k], split_axis=0, concat_axis=0)  8.7 us
    dot_general x1, matrix products, local(): lowered = jnp.dot(inner, down_whole, preferred_element_type=jnp.float32)  7.42 us
  transfers between devices with their start and end apart: 6, of which 2 were waited for; matrix products, arithmetic and copies ran while one was open for 14% of the time, Pallas kernels for 0%

profile of v1, /device:TPU:1, one launch (start us, length us, event | category | flops | bytes accessed | tf_op | source)
XLA Modules:
  0.0 303.5 jit_solution(6444988574333195931)
XLA Ops:
  6.5 1.4 divide_multiply_fusion
  8.0 1.0 log1p.7
  8.9 0.8 copy.47
  9.7 1.2 broadcast_add_fusion
  11.1 0.8 rev.17
  11.9 1.1 fusion.276
  13.0 0.6 slice_bitcast_fusion.35
  13.6 4.7 %all_gather.62 = bf16[2,4,128]{2,1,0:T(4,128)(2,1)S(1)} all-gather(bf16[1,4,128]{2,1,0:T(4,128)(2,1)S(1)} %get-tuple-element.86), channel_id=1, replica_groups=mesh['sp_0'=8,'sp_1'=4,'sp_2'=2,'tp'=4] {'sp_2'}, dimensions={0}, use_global_device_ids=true | all-gather | bytes 3072 | tf_op jit(solution)/shard_map/all_gather | solution.py:58
  18.2 0.6 fusion.242
  18.8 0.7 fusion.275
  19.6 0.8 squeeze.39
  20.3 1.0 fusion.40
  21.3 0.8 squeeze.37
  22.1 1.7 squeeze.43
  24.0 6.5 %all_gather.63 = bf16[4,4,128]{2,1,0:T(4,128)(2,1)S(1)} all-gather(bf16[1,4,128]{2,1,0:T(4,128)(2,1)} %fusion.242), channel_id=1, replica_groups=mesh['sp_0'=8,'sp_1'=4,'sp_2'=2,'tp'=4] {'sp_1'}, dimensions={0}, use_global_device_ids=true | all-gather | bytes 5120 | tf_op jit(solution)/shard_map/all_gather | solution.py:58
  30.5 2.5 exponential_multiply_fusion.3
  33.0 0.6 fusion.16
  33.7 3.8 %all-gather.1 = bf16[8,128,128]{2,1,0:T(8,128)(2,1)S(1)} all-gather(bf16[4,128,128]{2,1,0:T(8,128)(2,1)S(1)} %fusion.16), channel_id=3, replica_groups=mesh['sp_0'=8,'sp_1'=4,'sp_2'=2,'tp'=4] {'sp_2'}, dimensions={0}, use_global_device_ids=true | all-gather | bytes 393216 | tf_op jit(solution)/shard_map/all_gather | solution.py:58
  37.5 0.6 fusion.251
  38.2 0.2 fusion.88
  38.4 9.9 %all_gather.67 = bf16[4,4,128,128]{3,2,1,0:T(8,128)(2,1)S(1)} all-gather(bf16[1,4,128,128]{3,2,1,0:T(8,128)(2,1)S(1)} %fusion.88), channel_id=1, replica_groups=mesh['sp_0'=8,'sp_1'=4,'sp_2'=2,'tp'=4] {'sp_1'}, dimensions={0}, use_global_device_ids=true | all-gather | bytes 655360 | tf_op jit(solution)/shard_map/all_gather | solution.py:58
  48.3 1.0 fusion.74
  49.4 5.4 %all_gather.55 = bf16[2,4,128]{2,1,0:T(4,128)(2,1)S(1)} all-gather(bf16[1,4,128]{2,1,0:T(4,128)(2,1)} %get-tuple-element.113), channel_id=1, replica_groups=mesh['sp_0'=8,'sp_1'=4,'sp_2'=2,'tp'=4] {'sp_2'}, dimensions={0}, use_global_device_ids=true | all-gather | bytes 3072 | tf_op jit(solution)/shard_map/all_gather | solution.py:58
  54.9 5.4 %all_gather.56 = bf16[4,4,128]{2,1,0:T(4,128)(2,1)S(1)} all-gather(bf16[1,4,128]{2,1,0:T(4,128)(2,1)S(1)} %fusion.240), channel_id=1, replica_groups=mesh['sp_0'=8,'sp_1'=4,'sp_2'=2,'tp'=4] {'sp_1'}, dimensions={0}, use_global_device_ids=true | all-gather | bytes 5120 | tf_op jit(solution)/shard_map/all_gather | solution.py:58
  60.2 0.7 exponential_multiply_fusion.7
  60.9 1.4 fusion.15
  62.3 3.6 %all-gather = bf16[8,128,128]{2,1,0:T(8,128)(2,1)S(1)} all-gather(bf16[4,128,128]{2,1,0:T(8,128)(2,1)S(1)} %fusion.15), channel_id=2, replica_groups=mesh['sp_0'=8,'sp_1'=4,'sp_2'=2,'tp'=4] {'sp_2'}, dimensions={0}, use_global_device_ids=true | all-gather | bytes 393216 | tf_op jit(solution)/shard_map/all_gather | solution.py:58
  65.9 0.7 fusion.246
  66.8 10.7 %all_gather.60 = bf16[4,4,128,128]{3,2,1,0:T(8,128)(2,1)S(1)} all-gather(bf16[1,4,128,128]{3,2,1,0:T(8,128)(2,1)S(1)} %fusion.84), channel_id=1, replica_groups=mesh['sp_0'=8,'sp_1'=4,'sp_2'=2,'tp'=4] {'sp_1'}, dimensions={0}, use_global_device_ids=true | all-gather | bytes 655360 | tf_op jit(solution)/shard_map/all_gather | solution.py:58
  77.6 0.7 copy-done.1
  78.3 1.0 fusion.56
  79.4 1.6 pad_maximum_fusion.1
  81.0 1.7 stack.9
  82.7 4.1 %all-to-all-start.2 = ((bf16[4,1,1408,32]{2,3,1,0:T(8,128)(2,1)}), bf16[4,1,1408,32]{2,3,1,0:T(8,128)(2,1)}, u32[]{:S(2)}, u32[]{:S(2)}) async-start(bf16[4,1,1408,32]{2,3,1,0:T(8,128)(2,1)} %stack.9), calls=%async_computation.2 | async-start | bytes 720896 | tf_op jit(solution)/shard_map/all_to_all | solution.py:34
  86.8 1.2 convert_element_type.813
  88.0 15.6 %all_gather.64 = bf16[8,4,128]{2,1,0:T(4,128)(2,1)S(1)} all-gather(bf16[1,4,128]{2,1,0:T(4,128)(2,1)S(1)} %fusion.252), channel_id=1, replica_groups=mesh['sp_0'=8,'sp_1'=4,'sp_2'=2,'tp'=4] {'sp_0'}, dimensions={0}, use_global_device_ids=true | all-gather | bytes 9216 | tf_op jit(solution)/shard_map/all_gather | solution.py:58
  103.6 10.3 %all_gather.57 = bf16[8,4,128]{2,1,0:T(4,128)(2,1)S(1)} all-gather(bf16[1,4,128]{2,1,0:T(4,128)(2,1)S(1)} %fusion.247), channel_id=1, replica_groups=mesh['sp_0'=8,'sp_1'=4,'sp_2'=2,'tp'=4] {'sp_0'}, dimensions={0}, use_global_device_ids=true | all-gather | bytes 9216 | tf_op jit(solution)/shard_map/all_gather | solution.py:58
  114.0 0.6 fusion.259
  114.6 0.6 fusion.266
  115.2 1.6 convolution_select_fusion.1
  116.8 0.4 convolution_bitcast_fusion.5
  117.3 1.6 convolution_select_fusion
  118.9 0.6 convolution_bitcast_fusion.2
  119.5 1.4 fusion.11
  120.9 1.4 fusion.14
  122.3 4.2 %fusion.10 = f32[128,4,128]{0,2,1:T(8,128)} fusion(f32[128,4,128]{0,2,1:T(8,128)} %fusion.11, f32[128,4,128]{2,1,0:T(4,128)S(1)} %get-tuple-element.68, bf16[8,4,128,128]{3,2,1,0:T(8,128)(2,1)} %all-gather.8.cloned.1.call-done, f32[4,128]{1,0:T(4,128)S(1)} %get-tuple-element.110, f32[4,128]{1,0:T(4,128)} %copy-done.7, f32[4,128]{1,0:T(4,128)} %copy-done.9, ...), kind=kOutput, calls=%fused_computation.10 | convolution fusion | flops 104464384 | bytes 2654222 | tf_op jit(solution)/shard_map/thd,hdv->thv/dot_general | solution.py:201
  126.5 1.9 rev.20
  128.5 3.7 %multiply_reduce_fusion = (f32[128,4]{0,1:T(4,128)S(1)}, f32[128,4,128]{0,2,1:T(8,128)S(1)}) fusion(f32[128,4,128]{0,2,1:T(8,128)S(1)} %rev.20, f32[128,4,128]{0,2,1:T(8,128)} %fusion.14, f32[128,4,128]{2,1,0:T(4,128)S(1)} %get-tuple-element.67, bf16[8,4,128,128]{3,2,1,0:T(8,128)(2,1)} %all-gather.6.cloned.1.call-done, ...), kind=kOutput, calls=%fused_computation.172 | convolution fusion | flops 104660480 | bytes 2918414 | tf_op jit(solution)/shard_map/thd,hdv->thv/dot_general | solution.py:198
  132.5 1.4 convolution_convert_fusion
  133.9 10.7 %all_to_all.30 = bf16[4,32,2048]{2,1,0:T(8,128)(2,1)S(1)} all-to-all(bf16[4,32,2048]{2,1,0:T(8,128)(2,1)S(1)} %bitcast.514), channel_id=1, replica_groups=mesh['sp_0'=8,'sp_1'=4,'sp_2'=2,'tp'=4] {'tp'}, dimensions={0} | all-to-all | bytes 1048576 | tf_op jit(solution)/shard_map/all_to_all | solution.py:81
  144.6 2.9 stack.10
  147.5 4.6 %all-to-all-start.3 = ((bf16[8,4,1408,32]{2,3,1,0:T(8,128)(2,1)}), bf16[8,4,1408,32]{2,3,1,0:T(8,128)(2,1)}, u32[]{:S(2)}, u32[]{:S(2)}) async-start(bf16[8,4,1408,32]{2,3,1,0:T(8,128)(2,1)} %stack.10), calls=%async_computation.3 | async-start | bytes 5767168 | tf_op jit(solution)/shard_map/all_to_all | solution.py:34
  152.2 1.1 fusion.89
  153.4 78.6 %all-to-all-done.3 = bf16[8,4,1408,32]{2,3,1,0:T(8,128)(2,1)} async-done(((bf16[8,4,1408,32]{2,3,1,0:T(8,128)(2,1)}), bf16[8,4,1408,32]{2,3,1,0:T(8,128)(2,1)}, u32[]{:S(2)}, u32[]{:S(2)}) %all-to-all-start.3) | async-done | bytes 2883616 | tf_op jit(solution)/shard_map/all_to_all | solution.py:34
  232.0 3.3 %pad_maximum_fusion = bf16[2,32,1408,32]{2,3,1,0:T(8,128)(2,1)S(1)} fusion(bf16[1,32,1408,32]{2,3,1,0:T(8,128)(2,1)} %bitcast.70), kind=kLoop, calls=%fused_computation.4 | loop fusion | flops 2883584 | bytes 8650752 | tf_op jit(solution)/shard_map/stack | solution.py:33
  235.3 24.7 %all_to_all.31 = bf16[2,32,1408,32]{2,3,1,0:T(8,128)(2,1)} all-to-all(bf16[2,32,1408,32]{2,3,1,0:T(8,128)(2,1)S(1)} %pad_maximum_fusion), channel_id=1, replica_groups=mesh['sp_0'=8,'sp_1'=4,'sp_2'=2,'tp'=4] {'sp_2'}, dimensions={0} | all-to-all | bytes 11534336 | tf_op jit(solution)/shard_map/all_to_all | solution.py:34
  260.0 0.9 broadcast_in_dim.63
  260.9 3.5 %all-to-all-start.1 = ((bf16[4,32,2048]{2,1,0:T(8,128)(2,1)}), bf16[4,32,2048]{2,1,0:T(8,128)(2,1)S(1)}, u32[]{:S(2)}, u32[]{:S(2)}) async-start(bf16[4,32,2048]{2,1,0:T(8,128)(2,1)} %broadcast_in_dim.63), calls=%async_computation.1 | async-start | bytes 1048576 | tf_op jit(solution)/shard_map/all_to_all | solution.py:87
  264.4 6.0 %copy.67 = bf16[2,32,1408,32]{2,3,0,1:T(8,128)(2,1)} copy(bf16[2,32,1408,32]{2,3,1,0:T(8,128)(2,1)} %all_to_all.31) | data formatting | bytes 11534336 | tf_op jit(solution)/shard_map/all_to_all | solution.py:34
  270.3 3.2 %all-to-all-done.1 = bf16[4,32,2048]{2,1,0:T(8,128)(2,1)S(1)} async-done(((bf16[4,32,2048]{2,1,0:T(8,128)(2,1)}), bf16[4,32,2048]{2,1,0:T(8,128)(2,1)S(1)}, u32[]{:S(2)}, u32[]{:S(2)}) %all-to-all-start.1) | async-done | bytes 524320 | tf_op jit(solution)/shard_map/all_to_all | solution.py:87
  273.5 4.5 %fusion.2 = f32[128,1408]{1,0:T(8,128)} fusion(bf16[128,2048]{1,0:T(8,128)(2,1)S(1)} %bitcast.512, bf16[2048,2816]{1,0:T(8,128)(2,1)} %all-gather.10.cloned.1.call-done), kind=kOutput, calls=%fused_computation.2 | convolution fusion | flops 738197504 | bytes 7012352 | tf_op jit(solution)/shard_map/dot_general | solution.py:221
  278.1 7.4 %convolution_convert_fusion.1 = bf16[128,2048]{1,0:T(8,128)(2,1)S(1)} fusion(bf16[1408,2048]{0,1:T(8,128)(2,1)} %bitcast.510, bf16[128,2048]{1,0:T(8,128)(2,1)S(1)} %bitcast.513, bf16[2048,2816]{1,0:T(8,128)(2,1)} %all-gather.10.cloned.1.call-done, f32[128,1408]{1,0:T(8,128)} %fusion.2), kind=kOutput, calls=%fused_computation.8 | convolution fusion | flops 1477738496 | bytes 13303808 | tf_op jit(solution)/shard_map/dot_general | solution.py:224
  285.5 10.8 %all_to_all.32 = bf16[4,32,2048]{2,1,0:T(8,128)(2,1)S(1)} all-to-all(bf16[4,32,2048]{2,1,0:T(8,128)(2,1)S(1)} %bitcast.515), channel_id=1, replica_groups=mesh['sp_0'=8,'sp_1'=4,'sp_2'=2,'tp'=4] {'tp'}, dimensions={0} | all-to-all | bytes 1048576 | tf_op jit(solution)/shard_map/all_to_all | solution.py:81
  296.3 0.7 fusion.92
  (85 shorter events, 1.4 us)
Async XLA Ops:
  6.5 125.9 %copy-start = (bf16[512,2048]{1,0:T(8,128)(2,1)S(1)}, bf16[512,2048]{1,0:T(8,128)(2,1)}, u32[]{:S(2)}) copy-start(bf16[512,2048]{1,0:T(8,128)(2,1)} %param.20) | copy-start | bytes 6291460
  6.5 17.3 %copy-start.2 = (bf16[128,512]{1,0:T(8,128)(2,1)S(1)}, bf16[128,512]{1,0:T(8,128)(2,1)}, u32[]{:S(2)}) copy-start(bf16[128,512]{1,0:T(8,128)(2,1)} %param.15) | copy-start | bytes 393220
  6.5 115.7 %all-gather.8.cloned.1.call-start = ((), (), s32[]{:S(2)}) async-start(), calls=%async_computation.7 | async-start | bytes 1179648 | tf_op jit(solution)/shard_map/all_gather | solution.py:58
  11.1 27.1 %copy-start.3 = (f32[128,4,128]{2,1,0:T(4,128)}, f32[128,4,128]{2,1,0:T(4,128)S(1)}, u32[]{:S(2)}) copy-start(f32[128,4,128]{2,1,0:T(4,128)S(1)} %fusion.93) | copy-start | bytes 786436
  18.8 47.1 %copy-start.7 = (f32[4,128]{1,0:T(4,128)}, f32[4,128]{1,0:T(4,128)S(1)}, u32[]{:S(2)}) copy-start(f32[4,128]{1,0:T(4,128)S(1)} %convert_bitcast_fusion.20) | copy-start | bytes 6148
  30.5 17.8 %copy-start.11 = (f32[4,128]{1,0:T(4,128)}, f32[4,128]{1,0:T(4,128)S(1)}, u32[]{:S(2)}) copy-start(f32[4,128]{1,0:T(4,128)S(1)} %get-tuple-element.106) | copy-start | bytes 6148
  30.5 17.8 %copy-start.12 = (f32[4,128]{1,0:T(4,128)}, f32[4,128]{1,0:T(4,128)S(1)}, u32[]{:S(2)}) copy-start(f32[4,128]{1,0:T(4,128)S(1)} %get-tuple-element.107) | copy-start | bytes 6148
  30.5 17.8 %copy-start.13 = (f32[4,128]{1,0:T(4,128)}, f32[4,128]{1,0:T(4,128)S(1)}, u32[]{:S(2)}) copy-start(f32[4,128]{1,0:T(4,128)S(1)} %get-tuple-element.108) | copy-start | bytes 6148
  37.5 0.7 copy-start.4
  38.1 10.2 %copy-start.9 = (f32[4,128]{1,0:T(4,128)}, f32[4,128]{1,0:T(4,128)S(1)}, u32[]{:S(2)}) copy-start(f32[4,128]{1,0:T(4,128)S(1)} %get-tuple-element.105) | copy-start | bytes 6148
  49.4 79.1 %all-gather.6.cloned.1.call-start = ((), (), s32[]{:S(2)}) async-start(), calls=%async_computation.6 | async-start | bytes 1179648 | tf_op jit(solution)/shard_map/all_gather | solution.py:58
  65.9 0.7 copy-start.5
  65.9 11.6 %copy-start.8 = (f32[4,128]{1,0:T(4,128)}, f32[4,128]{1,0:T(4,128)S(1)}, u32[]{:S(2)}) copy-start(f32[4,128]{1,0:T(4,128)S(1)} %convert_bitcast_fusion.22) | copy-start | bytes 6148
  66.6 11.0 %copy-start.10 = (f32[4,128]{1,0:T(4,128)}, f32[4,128]{1,0:T(4,128)S(1)}, u32[]{:S(2)}) copy-start(f32[4,128]{1,0:T(4,128)S(1)} %get-tuple-element.101) | copy-start | bytes 6148
  77.5 0.8 copy-start.1
  77.5 0.8 copy-start.14
  77.5 0.8 copy-start.15
  77.6 0.8 copy-start.16
  79.3 194.2 %all-gather.10.cloned.1.call-start = ((), (), s32[]{:S(2)}) async-start(), calls=%async_computation.8 | async-start | bytes 11714560 | tf_op jit(solution)/shard_map/all_gather | solution.py:16
  82.7 51.2 %all-to-all-start.2 = ((bf16[4,1,1408,32]{2,3,1,0:T(8,128)(2,1)}), bf16[4,1,1408,32]{2,3,1,0:T(8,128)(2,1)}, u32[]{:S(2)}, u32[]{:S(2)}) async-start(bf16[4,1,1408,32]{2,3,1,0:T(8,128)(2,1)} %stack.9), calls=%async_computation.2 | async-start | bytes 720896 | tf_op jit(solution)/shard_map/all_to_all | solution.py:34
  117.3 11.2 %copy-start.18 = (f32[4,128]{1,0:T(4,128)S(1)}, f32[4,128]{1,0:T(4,128)}, u32[]{:S(2)}) copy-start(f32[4,128]{1,0:T(4,128)} %get-tuple-element.87) | copy-start | bytes 6148
  117.3 11.2 %copy-start.19 = (f32[4,128]{1,0:T(4,128)S(1)}, f32[4,128]{1,0:T(4,128)}, u32[]{:S(2)}) copy-start(f32[4,128]{1,0:T(4,128)} %get-tuple-element.88) | copy-start | bytes 6148
  117.3 11.2 %copy-start.20 = (f32[4,128]{1,0:T(4,128)S(1)}, f32[4,128]{1,0:T(4,128)}, u32[]{:S(2)}) copy-start(f32[4,128]{1,0:T(4,128)} %get-tuple-element.89) | copy-start | bytes 6148
  117.3 11.2 %copy-start.21 = (f32[4,128]{1,0:T(4,128)S(1)}, f32[4,128]{1,0:T(4,128)}, u32[]{:S(2)}) copy-start(f32[4,128]{1,0:T(4,128)} %get-tuple-element.90) | copy-start | bytes 6148
  117.3 11.2 %copy-start.22 = (f32[4,128]{1,0:T(4,128)S(1)}, f32[4,128]{1,0:T(4,128)}, u32[]{:S(2)}) copy-start(f32[4,128]{1,0:T(4,128)} %get-tuple-element.91) | copy-start | bytes 6148
  117.3 11.2 %copy-start.23 = (f32[4,128]{1,0:T(4,128)S(1)}, f32[4,128]{1,0:T(4,128)}, u32[]{:S(2)}) copy-start(f32[4,128]{1,0:T(4,128)} %get-tuple-element.92) | copy-start | bytes 6148
  117.3 11.2 %copy-start.24 = (f32[4,128]{1,0:T(4,128)S(1)}, f32[4,128]{1,0:T(4,128)}, u32[]{:S(2)}) copy-start(f32[4,128]{1,0:T(4,128)} %get-tuple-element.93) | copy-start | bytes 6148
  119.5 9.0 %copy-start.6 = (bf16[8,128,128]{2,1,0:T(8,128)(2,1)S(1)}, bf16[8,128,128]{2,1,0:T(8,128)(2,1)}, u32[]{:S(2)}) copy-start(bf16[8,128,128]{2,1,0:T(8,128)(2,1)} %copy-done.5) | copy-start | bytes 786436
  120.9 11.3 %copy-start.25 = (f32[128]{0:T(128)S(1)}, f32[128]{0:T(128)}, u32[]{:S(2)}) copy-start(f32[128]{0:T(128)} %convert_element_type.813) | copy-start | bytes 1540
  133.8 18.2 %copy-start.17 = (bf16[2048]{0:T(1024)(128)(2,1)S(1)}, bf16[2048]{0:T(1024)(128)(2,1)}, u32[]{:S(2)}) copy-start(bf16[2048]{0:T(1024)(128)(2,1)} %param.22) | copy-start | bytes 12292
  147.5 84.5 %all-to-all-start.3 = ((bf16[8,4,1408,32]{2,3,1,0:T(8,128)(2,1)}), bf16[8,4,1408,32]{2,3,1,0:T(8,128)(2,1)}, u32[]{:S(2)}, u32[]{:S(2)}) async-start(bf16[8,4,1408,32]{2,3,1,0:T(8,128)(2,1)} %stack.10), calls=%async_computation.3 | async-start | bytes 5767168 | tf_op jit(solution)/shard_map/all_to_all | solution.py:34
  260.9 12.6 %all-to-all-start.1 = ((bf16[4,32,2048]{2,1,0:T(8,128)(2,1)}), bf16[4,32,2048]{2,1,0:T(8,128)(2,1)S(1)}, u32[]{:S(2)}, u32[]{:S(2)}) async-start(bf16[4,32,2048]{2,1,0:T(8,128)(2,1)} %broadcast_in_dim.63), calls=%async_computation.1 | async-start | bytes 1048576 | tf_op jit(solution)/shard_map/all_to_all | solution.py:87
Sparse Core Ops, SparseCore 0:
  49.5 37.8 all-gather.7
  89.1 36.8 all-gather.5
  128.7 122.8 all-gather.9
